TPU v7x, 32 devices: a whole 2x2x4 slice. The times are simulated.
32 devices in a mesh: grp: 2 (over y), sp: 4 (over z), tp: 4 (over x, core).
Axes of the slice: x: 2, y: 2, z: 4, core: 2. Of those that a mesh axis runs over, the one named last changes fastest.
Arguments:
- inputs: bfloat16 [2048, 2048], P(('grp', 'sp')), parts along dimension 0, may hold values from -6 to 6
- norm_gain: float32 [2048], replicated, may hold values from 0.1 to 1.9
- da_query_weight: bfloat16 [2048, 1024], P('sp', 'tp'), may hold values from -0.125 to 0.125
- da_key_weight: bfloat16 [2048, 1024], P('sp', 'tp'), may hold values from -0.125 to 0.125
- da_value_weight: bfloat16 [2048, 1024], P('sp', 'tp'), may hold values from -0.125 to 0.125
- sw_query_weight: bfloat16 [2048, 1024], P('sp', 'tp'), may hold values from -0.125 to 0.125
- sw_key_weight: bfloat16 [2048, 512], P('sp', 'tp'), may hold values from -0.125 to 0.125
- sw_value_weight: bfloat16 [2048, 512], P('sp', 'tp'), may hold values from -0.125 to 0.125
- da_query_gain: float32 [64], replicated, may hold values from 0.6 to 30
- da_key_gain: float32 [64], replicated, may hold values from 0.6 to 30
- sw_query_gain: float32 [64], replicated, may hold values from 0.6 to 30
- sw_key_gain: float32 [64], replicated, may hold values from 0.6 to 30
- mix_lambda: float32 [8], P('tp'), may hold values from 0.3 to 0.8
- head_gain: float32 [128], replicated, may hold values from 0.1 to 1.9
- sink_logit: float32 [16], P('tp'), may hold values from 0 to 8
- da_out_weight: bfloat16 [1024, 2048], P('tp'), may hold values from -0.1875 to 0.1875
- sw_out_weight: bfloat16 [1024, 2048], P('tp'), may hold values from -0.1875 to 0.1875
Outputs:
- mixed: bfloat16 [2048, 2048], P(('grp', 'sp')), parts along dimension 0
There are 2 independent parts, one for each index of `grp`. A program takes and returns all parts, laid end to end along the dimension named above; an argument that names none is the same for every part. Nothing has to cross between parts.
All inputs are finite; a program needn't handle non-finite values.
Results may differ from a plain program's by a relative error of at most 0.014.
The roundings to bfloat16 on the way count: a program that leaves them out, or rounds other values in their place, can miss the bound.
Values may be sent and summed in bfloat16 or wider, within the bound.
A program may use at most 64 MiB of HBM per device.

v0:
```python
import jax
import jax.numpy as jnp
from jax import lax
from jax.sharding import PartitionSpec as P

HD = 64
WINDOW = 128


def shifted(value, axis, steps):
    count = lax.axis_size(axis)
    first, last = (max(0, -steps), min(count, count - steps))
    return lax.ppermute(value, axis, [(source, source + steps) for source in range(first, last)])


def rms_norm(values, gain):
    return values * lax.rsqrt(jnp.mean(values * values, axis=-1, keepdims=True) + 1e-06) * gain


def absorb(state, queries, places, keys, values, key_places):
    top, total, summed = state
    scores = jnp.einsum(
        "qhmd,khmd->hmqk", queries, keys, preferred_element_type=jnp.float32
    ) * HD ** (-0.5)
    scores = jnp.where(key_places[None, :] <= places[:, None], scores, -jnp.inf)
    new_top = jnp.maximum(top, jnp.max(scores, axis=-1))
    weights = jnp.exp(scores - new_top[..., None])
    total = jnp.sum(weights, axis=-1)
    summed = jnp.einsum(
        "hmqk,khe->hmqe", weights.astype(jnp.bfloat16), values, preferred_element_type=jnp.float32
    )
    return (new_top, total, summed)


def keep(state, queries, places, keys, values, key_places):
    return state


def diff_attention(queries, places, da_key, da_value, mix_lambda, head_gain):
    rows = queries.shape[0]
    heads = queries.shape[1]
    half = rows // 2
    fresh = (
        jnp.full((heads, 2, half), -1e30, jnp.float32),
        jnp.zeros((heads, 2, half), jnp.float32),
        jnp.zeros((heads, 2, half, 2 * HD), jnp.float32),
    )
    states = (fresh, fresh)
    start = jnp.int32(0)
    keys = lax.all_gather(da_key, "sp", axis=0, tiled=True)
    values = lax.all_gather(da_value, "sp", axis=0, tiled=True)
    key_places = jnp.arange(keys.shape[0], dtype=jnp.int32)
    updated = []
    for section in range(2):
        own_rows = queries[section * half : (section + 1) * half]
        own_places = places[section * half : (section + 1) * half]
        updated.append(
            lax.cond(
                start <= jnp.max(own_places),
                absorb,
                keep,
                states[section],
                own_rows,
                own_places,
                keys,
                values,
                key_places,
            )
        )
    states = tuple(updated)
    blended = []
    for top, total, summed in states:
        maps = summed / total[..., None]
        blended.append(maps[:, 0] - mix_lambda[:, None, None] * maps[:, 1])
    blend = jnp.transpose(jnp.concatenate(blended, axis=1), (1, 0, 2))
    return rms_norm(blend, head_gain).astype(jnp.bfloat16).reshape(rows, heads * 2 * HD)


def window_attention(sw_query, sw_key, sw_value, earlier_key, earlier_value, sink_logit, first):
    rows = sw_query.shape[0]
    sw_heads = sw_query.shape[1]
    kv_heads = sw_key.shape[1]
    groups = sw_heads // kv_heads
    count = rows // WINDOW

    def band(own, earlier_tile):
        tiles = own.reshape(count, WINDOW, kv_heads, HD)
        earlier = jnp.concatenate([earlier_tile[None], tiles[:-1]], axis=0)
        return jnp.concatenate([earlier, tiles], axis=1)

    key_band = band(sw_key, earlier_key)
    value_band = band(sw_value, earlier_value)
    query_tiles = sw_query.reshape(count, WINDOW, kv_heads, groups, HD)
    scores = jnp.einsum(
        "nqhgd,nkhd->nhgqk", query_tiles, key_band, preferred_element_type=jnp.float32
    ) * HD ** (-0.5)
    lag = WINDOW + jnp.arange(WINDOW)[:, None] - jnp.arange(2 * WINDOW)[None, :]
    key_places = (
        first + jnp.arange(count)[:, None] * WINDOW - WINDOW + jnp.arange(2 * WINDOW)[None, :]
    )
    valid = ((lag >= 0) & (lag < WINDOW))[None] & (key_places >= 0)[:, None, :]
    scores = jnp.where(valid[:, None, None], scores, -jnp.inf)
    sink = sink_logit.reshape(kv_heads, groups)[None, :, :, None]
    top = jnp.maximum(jnp.max(scores, axis=-1), sink)
    weights = jnp.exp(scores - top[..., None])
    total = jnp.sum(weights, axis=-1) + jnp.exp(sink - top)
    summed = jnp.einsum(
        "nhgqk,nkhd->nqhgd",
        weights.astype(jnp.bfloat16),
        value_band,
        preferred_element_type=jnp.float32,
    )
    return (
        (summed / jnp.transpose(total, (0, 3, 1, 2))[..., None])
        .astype(jnp.bfloat16)
        .reshape(rows, sw_heads * HD)
    )


def on_device(
    inputs,
    norm_gain,
    da_query_weight,
    da_key_weight,
    da_value_weight,
    sw_query_weight,
    sw_key_weight,
    sw_value_weight,
    da_query_gain,
    da_key_gain,
    sw_query_gain,
    sw_key_gain,
    mix_lambda,
    head_gain,
    sink_logit,
    da_out_weight,
    sw_out_weight,
):
    rows = inputs.shape[0]
    normed = rms_norm(inputs.astype(jnp.float32), norm_gain).astype(jnp.bfloat16)
    pieces = (
        lax.all_gather(da_query_weight, "sp", axis=0, tiled=True),
        lax.all_gather(da_key_weight, "sp", axis=0, tiled=True),
        lax.all_gather(da_value_weight, "sp", axis=0, tiled=True),
        lax.all_gather(sw_query_weight, "sp", axis=0, tiled=True),
        lax.all_gather(sw_key_weight, "sp", axis=0, tiled=True),
        lax.all_gather(sw_value_weight, "sp", axis=0, tiled=True),
    )
    projected = tuple(
        (jnp.dot(normed, piece, preferred_element_type=jnp.float32) for piece in pieces)
    )
    da_heads = da_query_weight.shape[1] // (2 * HD)
    sw_heads = sw_query_weight.shape[1] // HD
    kv_heads = sw_key_weight.shape[1] // HD
    da_query = rms_norm(projected[0].reshape(rows, da_heads, 2, HD), da_query_gain).astype(
        jnp.bfloat16
    )
    da_key = rms_norm(projected[1].reshape(rows, da_heads, 2, HD), da_key_gain).astype(jnp.bfloat16)
    da_value = projected[2].astype(jnp.bfloat16).reshape(rows, da_heads, 2 * HD)
    sw_query = rms_norm(projected[3].reshape(rows, sw_heads, HD), sw_query_gain).astype(
        jnp.bfloat16
    )
    sw_key = rms_norm(projected[4].reshape(rows, kv_heads, HD), sw_key_gain).astype(jnp.bfloat16)
    sw_value = projected[5].astype(jnp.bfloat16).reshape(rows, kv_heads, HD)
    place = lax.axis_index("sp")
    first = place * rows
    earlier_key, earlier_value = shifted(
        (sw_key[rows - WINDOW :], sw_value[rows - WINDOW :]), "sp", 1
    )
    sw_rows = window_attention(
        sw_query, sw_key, sw_value, earlier_key, earlier_value, sink_logit, first
    )
    places = first + jnp.arange(rows, dtype=jnp.int32)
    da_rows = diff_attention(da_query, places, da_key, da_value, mix_lambda, head_gain)
    partial_value = jnp.dot(da_rows, da_out_weight, preferred_element_type=jnp.float32) + jnp.dot(
        sw_rows, sw_out_weight, preferred_element_type=jnp.float32
    )
    return lax.psum(partial_value.astype(jnp.bfloat16), "tp")


def solution(mesh):
    return jax.shard_map(
        on_device,
        mesh=mesh,
        in_specs=(
            P(("grp", "sp"), None),
            P(),
            P("sp", "tp"),
            P("sp", "tp"),
            P("sp", "tp"),
            P("sp", "tp"),
            P("sp", "tp"),
            P("sp", "tp"),
            P(),
            P(),
            P(),
            P(),
            P("tp"),
            P(),
            P("tp"),
            P("tp", None),
            P("tp", None),
        ),
        out_specs=P(("grp", "sp"), None),
        check_vma=False,
    )
```

profile of v0, /device:TPU:0, one launch (start us, length us, event | category | flops | bytes accessed | tf_op | source)
XLA Modules:
  0.0 211.7 jit_solution(5717824083418548665)
XLA Ops:
  6.5 0.7 all-gather.9.cloned.1.call-update
  7.3 0.0 all-gather.7.cloned.1.call-start
  7.3 0.7 all-gather.7.cloned.1.call-update
  8.0 0.0 all-gather.5.cloned.1.call-start
  8.1 0.7 all-gather.5.cloned.1.call-update
  8.8 0.0 all-gather.11.cloned.1.call-start
  8.8 1.5 fusion.29
  10.4 22.7 %all_gather.30 = bf16[2048,128]{1,0:T(8,128)(2,1)S(1)} all-gather(bf16[512,128]{1,0:T(8,128)(2,1)} %param.27), channel_id=1, replica_groups=mesh['grp'=2,'sp'=4,'tp'=4] {'sp'}, dimensions={0}, use_global_device_ids=true | all-gather | bytes 655360 | tf_op jit(solution)/shard_map/all_gather | solution.py:146
  33.0 0.6 multiply_reduce_fusion.3
  33.7 0.1 multiply_convert_fusion.3
  33.7 0.6 fusion.78
  34.4 2.5 %collective-permute-start.1 = (bf16[128,2,64]{0,2,1:T(8,128)(2,1)}, bf16[128,2,64]{0,2,1:T(8,128)(2,1)S(1)}, u32[]{:S(2)}, u32[]{:S(2)}) collective-permute-start(bf16[128,2,64]{0,2,1:T(8,128)(2,1)} %get-tuple-element.55), channel_id=1, source_target_pairs={{0,4},{4,8},{8,12},{1,5},{5,9},{9,13},{2,6},{6,10},{10,14},{3,7},{... | collective-permute-start | bytes 98312 | tf_op jit(solution)/shard_map/ppermute | solution.py:13
  36.9 18.3 %all_gather.29 = bf16[2048,128]{1,0:T(8,128)(2,1)S(1)} all-gather(bf16[512,128]{1,0:T(8,128)(2,1)S(1)} %copy-done.3), channel_id=1, replica_groups=mesh['grp'=2,'sp'=4,'tp'=4] {'sp'}, dimensions={0}, use_global_device_ids=true | all-gather | bytes 655360 | tf_op jit(solution)/shard_map/all_gather | solution.py:147
  55.2 0.6 convolution_convert_fusion.1
  55.8 0.6 fusion.77
  56.4 1.9 collective-permute-start
  58.4 0.0 all-gather.11.cloned.1.call-update
  58.4 0.0 all-reduce.2.cloned.1.call-start
  58.5 0.1 reshape.180
  58.6 0.7 slice_reduce_fusion.1
  60.7 0.1 add_compare_fusion
  60.8 0.1 max.16
  60.9 0.6 copy.31
  61.5 0.1 fusion.58
  61.6 0.1 broadcast_and_fusion
  61.7 0.0 all-gather.9.cloned.1.call-done
  61.8 1.9 convolution_convert_fusion
  63.7 0.1 copy.26
  63.8 14.9 %all-gather.7.cloned.1.call-done = bf16[2048,256]{1,0:T(8,128)(2,1)} async-done(((bf16[512,256]{1,0:T(8,128)(2,1)}), bf16[2048,256]{1,0:T(8,128)(2,1)}) %all-gather.7.cloned.1.call-update) | async-done | bytes 1048592 | tf_op jit(solution)/shard_map/all_gather | solution.py:143
  78.7 1.9 multiply_reduce_fusion.1
  80.6 0.1 multiply_convert_fusion.1
  80.7 18.9 %all_gather.26 = bf16[1024,2,2,64]{0,3,2,1:T(8,128)(2,1)S(1)} all-gather(bf16[256,2,2,64]{0,3,2,1:T(8,128)(2,1)S(1)} %multiply_convert_fusion.1), channel_id=1, replica_groups=mesh['grp'=2,'sp'=4,'tp'=4] {'sp'}, dimensions={0}, use_global_device_ids=true | all-gather | bytes 655360 | tf_op jit(solution)/shard_map/all_gather | solution.py:50
  99.6 11.3 %all-gather.5.cloned.1.call-done = bf16[2048,256]{1,0:T(8,128)(2,1)} async-done(((bf16[512,256]{1,0:T(8,128)(2,1)}), bf16[2048,256]{1,0:T(8,128)(2,1)}) %all-gather.5.cloned.1.call-update) | async-done | bytes 1048592 | tf_op jit(solution)/shard_map/all_gather | solution.py:142
  110.9 1.9 multiply_reduce_fusion.2
  112.8 27.5 %all-gather.11.cloned.1.call-done = bf16[2048,256]{1,0:T(8,128)(2,1)} async-done(((bf16[512,256]{1,0:T(8,128)(2,1)}), bf16[2048,256]{1,0:T(8,128)(2,1)}) %all-gather.11.cloned.1.call-update) | async-done | bytes 1048592 | tf_op jit(solution)/shard_map/all_gather | solution.py:145
  140.4 1.9 bitcast_reduce_fusion
  142.3 0.1 multiply_convert_fusion.2
  142.4 15.3 %all_gather.28 = bf16[1024,2,128]{2,0,1:T(8,128)(2,1)S(1)} all-gather(bf16[256,2,128]{2,0,1:T(8,128)(2,1)S(1)} %copy.26), channel_id=1, replica_groups=mesh['grp'=2,'sp'=4,'tp'=4] {'sp'}, dimensions={0}, use_global_device_ids=true | all-gather | bytes 655360 | tf_op jit(solution)/shard_map/all_gather | solution.py:51
  157.7 2.3 %conditional.3 = (f32[2,2,128]{2,1,0:T(2,128)S(1)}, f32[2,2,128,128]{2,3,0,1:T(8,128)S(1)}) conditional(s32[]{:T(128)} %convert_element_type.58, () %tuple.23, (s32[1024]{0:T(1024)S(1)}, s32[128]{0:T(128)S(1)}, bf16[256,2,2,64]{0,3,2,1:T(8,128)(2,1)S(1)}, bf16[1024,2,2,64]{0,3,2,1:T(8,128)(2,1)S(1)}, bf16[1024,2,128]{2,0,1:T(8,128)(2,1)S(1)}) %tuple.24), branch_computations={%region_9.10_spmd, %region_10.13_spmd} | conditional | flops 207224320 | bytes 8733200 | solution.py:58
  157.7 0.1 broadcast_compare_fusion.1
  157.8 0.6 fusion.14
  158.4 0.6 fusion.16
  159.1 0.7 fusion.17
  159.8 0.1 copy.45
  160.0 2.3 %conditional.2 = (f32[2,2,128]{2,1,0:T(2,128)S(1)}, f32[2,2,128,128]{2,3,0,1:T(8,128)S(1)}) conditional(s32[]{:T(128)} %convert_element_type.52, () %tuple.21, (s32[1024]{0:T(1024)S(1)}, s32[128]{0:T(128)S(1)}, bf16[256,2,2,64]{0,3,2,1:T(8,128)(2,1)S(1)}, bf16[1024,2,2,64]{0,3,2,1:T(8,128)(2,1)S(1)}, bf16[1024,2,128]{2,0,1:T(8,128)(2,1)S(1)}) %tuple.22), branch_computations={%region_4.0_spmd, %region_5.8_spmd} | conditional | flops 207224320 | bytes 8733200 | solution.py:58
  160.0 0.1 broadcast_compare_fusion
  160.2 0.6 fusion
  160.8 0.6 fusion.2
  161.4 0.7 fusion.3
  162.1 0.1 copy.43
  162.3 0.1 reshape.181
  162.5 0.4 fusion.79
  162.9 0.1 broadcast_maximum_fusion.2
  163.0 0.2 fusion.36
  163.1 0.1 add_bitcast_fusion
  163.3 0.1 fusion.48
  163.5 0.3 fusion.35
  163.8 0.1 copy.36
  163.9 0.1 multiply_convert_fusion
  164.0 0.5 fusion.80
  164.5 0.5 copy-done.2
  165.0 1.4 fusion.28
  166.5 36.4 %all-reduce.2.cloned.1.call-done = bf16[256,2048]{1,0:T(8,128)(2,1)} async-done(((bf16[256,2048]{1,0:T(8,128)(2,1)}), bf16[256,2048]{1,0:T(8,128)(2,1)}) %all-reduce.2.cloned.1.call-update) | async-done | bytes 1048592 | tf_op jit(solution)/shard_map/psum | solution.py:178
  202.9 2.3 %copy.73 = bf16[256,2048]{1,0:T(8,128)(2,1)} copy(bf16[256,2048]{1,0:T(8,128)(2,1)} %all-reduce.2.cloned.1.call-done) | data formatting | bytes 2097152
  (52 shorter events, 0.3 us)
Async XLA Ops:
  6.5 157.5 %copy-start = (bf16[256,2048]{1,0:T(8,128)(2,1)S(1)}, bf16[256,2048]{1,0:T(8,128)(2,1)}, u32[]{:S(2)}) copy-start(bf16[256,2048]{1,0:T(8,128)(2,1)} %param.36) | copy-start | bytes 3145732
  6.5 26.5 %copy-start.1 = (bf16[256,2048]{1,0:T(8,128)(2,1)S(1)}, bf16[256,2048]{1,0:T(8,128)(2,1)}, u32[]{:S(2)}) copy-start(bf16[256,2048]{1,0:T(8,128)(2,1)} %param.21) | copy-start | bytes 3145732
  6.5 26.5 %copy-start.12 = (f32[2048]{0:T(1024)S(1)}, f32[2048]{0:T(1024)}, u32[]{:S(2)}) copy-start(f32[2048]{0:T(1024)} %param.22) | copy-start | bytes 24580
  6.5 55.2 %all-gather.9.cloned.1.call-start = ((), (), s32[]{:S(2)}) async-start(), calls=%async_computation.2 | async-start | bytes 1310720 | tf_op jit(solution)/shard_map/all_gather | solution.py:144
  7.3 71.5 %all-gather.7.cloned.1.call-start = ((), (), s32[]{:S(2)}) async-start(), calls=%async_computation.1 | async-start | bytes 1310720 | tf_op jit(solution)/shard_map/all_gather | solution.py:143
  8.0 25.6 %copy-start.7 = (f32[64]{0:T(128)S(1)}, f32[64]{0:T(128)}, u32[]{:S(2)}) copy-start(f32[64]{0:T(128)} %param.32) | copy-start | bytes 772
  8.0 102.9 %all-gather.5.cloned.1.call-start = ((), (), s32[]{:S(2)}) async-start(), calls=%async_computation | async-start | bytes 1310720 | tf_op jit(solution)/shard_map/all_gather | solution.py:142
  8.8 28.1 %copy-start.3 = (bf16[512,128]{1,0:T(8,128)(2,1)S(1)}, bf16[512,128]{1,0:T(8,128)(2,1)}, u32[]{:S(2)}) copy-start(bf16[512,128]{1,0:T(8,128)(2,1)} %param.28) | copy-start | bytes 393220
  8.8 131.6 %all-gather.11.cloned.1.call-start = ((), (), s32[]{:S(2)}) async-start(), calls=%async_computation.3 | async-start | bytes 1310720 | tf_op jit(solution)/shard_map/all_gather | solution.py:145
  33.6 27.2 %copy-start.13 = (f32[4]{0:T(128)S(1)}, f32[4]{0:T(128)}, u32[]{:S(2)}) copy-start(f32[4]{0:T(128)} %param.35) | copy-start | bytes 52
  34.4 128.1 %collective-permute-start.1 = (bf16[128,2,64]{0,2,1:T(8,128)(2,1)}, bf16[128,2,64]{0,2,1:T(8,128)(2,1)S(1)}, u32[]{:S(2)}, u32[]{:S(2)}) collective-permute-start(bf16[128,2,64]{0,2,1:T(8,128)(2,1)} %get-tuple-element.55), channel_id=1, source_target_pairs={{0,4},{4,8},{8,12},{1,5},{5,9},{9,13},{2,6},{6,10},{10,14},{3,7},{... | collective-permute-start | bytes 98312 | tf_op jit(solution)/shard_map/ppermute | solution.py:13
  56.4 107.0 %collective-permute-start = (bf16[128,2,64]{0,2,1:T(8,128)(2,1)}, bf16[128,2,64]{0,2,1:T(8,128)(2,1)S(1)}, u32[]{:S(2)}, u32[]{:S(2)}) collective-permute-start(bf16[128,2,64]{0,2,1:T(8,128)(2,1)} %bitcast.13), channel_id=1, source_target_pairs={{0,4},{4,8},{8,12},{1,5},{5,9},{9,13},{2,6},{6,10},{10,14},{3,7},{... | collective-permute-start | bytes 98312 | tf_op jit(solution)/shard_map/ppermute | solution.py:13
  58.4 144.5 %all-reduce.2.cloned.1.call-start = ((), (), s32[]{:S(2)}) async-start(), calls=%async_computation.4 | async-start | bytes 2097152 | tf_op jit(solution)/shard_map/psum | solution.py:178
  63.7 17.0 %copy-start.8 = (f32[64]{0:T(128)S(1)}, f32[64]{0:T(128)}, u32[]{:S(2)}) copy-start(f32[64]{0:T(128)} %param.30) | copy-start | bytes 772
  112.8 29.5 %copy-start.9 = (f32[64]{0:T(128)S(1)}, f32[64]{0:T(128)}, u32[]{:S(2)}) copy-start(f32[64]{0:T(128)} %param.29) | copy-start | bytes 772
  160.0 2.5 %copy-start.6 = (bf16[1,128,2,64]{1,3,2,0:T(8,128)(2,1)S(1)}, bf16[1,128,2,64]{1,3,2,0:T(8,128)(2,1)}, u32[]{:S(2)}) copy-start(bf16[1,128,2,64]{1,3,2,0:T(8,128)(2,1)} %get-tuple-element.56) | copy-start | bytes 98308
  160.0 2.5 %copy-start.14 = (f32[64]{0:T(128)S(1)}, f32[64]{0:T(128)}, u32[]{:S(2)}) copy-start(f32[64]{0:T(128)} %param.31) | copy-start | bytes 772
  162.3 1.0 copy-start.11
  162.5 1.0 copy-start.4
  162.5 1.0 copy-start.5
  163.2 0.7 copy-start.10
  163.8 1.2 copy-start.2
Sparse Core Ops, SparseCore 0:
  8.9 39.4 all-gather.8
  50.0 28.6 all-gather.6
  80.3 30.5 all-gather.4
  112.3 27.9 all-gather.10
  166.6 36.2 all-reduce.1
where the time goes:
time: 212 us
  waiting for transfers between devices  92.3 us (44%)
  blocking collectives  75.2 us (35%)
  between operations  14.9 us (7%)
  matrix products  14 us (7%)
  local copies, waits for them, and re-layouts  5.61 us (3%)
  other arithmetic  5.05 us (2%)
  starting transfers between devices  4.58 us (2%)
    psum x1, waiting for transfers between devices, on_device(): return lax.psum(partial_value.astype(jnp.bfloat16), 'tp')  36.4 us
    all_gather x1, waiting for transfers between devices, on_device(): lax.all_gather(sw_query_weight, 'sp', axis=0, tiled=True)  27.5 us
    all_gather x1, blocking collectives, on_device(): lax.all_gather(sw_key_weight, 'sp', axis=0, tiled=True)  22.7 us
    all_gather x1, blocking collectives, diff_attention(): keys = lax.all_gather(da_key, 'sp', axis=0, tiled=True)  18.9 us
    all_gather x1, blocking collectives, on_device(): lax.all_gather(sw_value_weight, 'sp', axis=0, tiled=True)  18.3 us
    all_gather x1, blocking collectives, diff_attention(): values = lax.all_gather(da_value, 'sp', axis=0, tiled=True)  15.3 us
    all_gather x1, waiting for transfers between devices, on_device(): lax.all_gather(da_key_weight, 'sp', axis=0, tiled=True)  14.9 us
    all_gather x1, waiting for transfers between devices, on_device(): lax.all_gather(da_query_weight, 'sp', axis=0, tiled=True)  11.3 us
  transfers between devices with their start and end apart: 7, of which 4 were waited for; matrix products, arithmetic and copies ran while one was open for 9% of the time, Pallas kernels for 0%

commit v1 on v0

--- a/solution.py
+++ b/solution.py
@@ -175,7 +175,7 @@
     partial_value = jnp.dot(da_rows, da_out_weight, preferred_element_type=jnp.float32) + jnp.dot(
         sw_rows, sw_out_weight, preferred_element_type=jnp.float32
     )
-    return lax.psum(partial_value.astype(jnp.bfloat16), "tp")
+    return jnp.sum(lax.all_gather(partial_value.astype(jnp.bfloat16), "tp"), axis=0)
 
 
 def solution(mesh):

time: 212 us -> 224 us (1.057)
  waiting for transfers between devices: 92.3 us -> 104 us
  other arithmetic: 5.05 us -> 11.1 us
  blocking collectives: 75.2 us -> 71.3 us
  local copies, waits for them, and re-layouts: 5.61 us -> 3.31 us
    psum x1 -> x0, waiting for transfers between devices: 36.4 us -> none  [on_device(): return lax.psum(partial_value.astype(jnp.bfloat16), 'tp')]
    all_gather x0 -> x1, waiting for transfers between devices: none -> 34.4 us  [on_device(): lax.all_gather(partial_value.astype(jnp.bfloat16), 'tp')]
    all_gather x1, waiting for transfers between devices: 0.02 us -> 26.9 us  [on_device(): lax.all_gather(da_value_weight, 'sp', axis=0, tiled=True)]
    all_gather x1, waiting for transfers between devices: 27.5 us -> 13.2 us  [on_device(): lax.all_gather(sw_query_weight, 'sp', axis=0, tiled=True)]
    all_gather x1, waiting for transfers between devices: 14.9 us -> 27.4 us  [on_device(): lax.all_gather(da_key_weight, 'sp', axis=0, tiled=True)]
    all_gather x1, waiting for transfers between devices: 11.3 us -> 0.01 us  [on_device(): lax.all_gather(da_query_weight, 'sp', axis=0, tiled=True)]
    reduce_sum x0 -> x1, other arithmetic: none -> 4.25 us  [on_device(): jnp.sum(lax.all_gather(partial_value.astype(jnp.bfloat16), 'tp'), axis=0)]
    all_gather x1, blocking collectives: 18.9 us -> 15 us  [diff_attention(): keys = lax.all_gather(da_key, 'sp', axis=0, tiled=True)]
where the time goes in v1:
time: 224 us
  waiting for transfers between devices  104 us (46%)
  blocking collectives  71.3 us (32%)
  between operations  15 us (7%)
  matrix products  14 us (6%)
  other arithmetic  11.1 us (5%)
  starting transfers between devices  4.58 us (2%)
  local copies, waits for them, and re-layouts  3.31 us (1%)
    all_gather x1, waiting for transfers between devices, on_device(): lax.all_gather(partial_value.astype(jnp.bfloat16), 'tp')  34.4 us
    all_gather x1, waiting for transfers between devices, on_device(): lax.all_gather(da_key_weight, 'sp', axis=0, tiled=True)  27.4 us
    all_gather x1, waiting for transfers between devices, on_device(): lax.all_gather(da_value_weight, 'sp', axis=0, tiled=True)  26.9 us
    all_gather x1, blocking collectives, on_device(): lax.all_gather(sw_key_weight, 'sp', axis=0, tiled=True)  22.7 us
    all_gather x1, blocking collectives, on_device(): lax.all_gather(sw_value_weight, 'sp', axis=0, tiled=True)  18.4 us
    all_gather x1, blocking collectives, diff_attention(): values = lax.all_gather(da_value, 'sp', axis=0, tiled=True)  15.3 us
    all_gather x1, blocking collectives, diff_attention(): keys = lax.all_gather(da_key, 'sp', axis=0, tiled=True)  15 us
    all_gather x1, waiting for transfers between devices, on_device(): lax.all_gather(sw_query_weight, 'sp', axis=0, tiled=True)  13.2 us
  transfers between devices with their start and end apart: 7, of which 4 were waited for; matrix products, arithmetic and copies ran while one was open for 9% of the time, Pallas kernels for 0%

profile of v1, /device:TPU:0, one launch (start us, length us, event | category | flops | bytes accessed | tf_op | source)
XLA Modules:
  0.0 223.6 jit_solution(8218282624736209519)
XLA Ops:
  6.5 0.7 all-gather.7.cloned.1.call-update
  7.3 0.0 all-gather.13.cloned.1.call-start
  7.3 0.7 all-gather.13.cloned.1.call-update
  8.0 0.0 all-gather.9.cloned.1.call-start
  8.1 0.7 all-gather.9.cloned.1.call-update
  8.8 0.0 all-gather.11.cloned.1.call-start
  8.8 1.5 fusion.29
  10.4 22.7 %all_gather.36 = bf16[2048,128]{1,0:T(8,128)(2,1)S(1)} all-gather(bf16[512,128]{1,0:T(8,128)(2,1)} %param.27), channel_id=1, replica_groups=mesh['grp'=2,'sp'=4,'tp'=4] {'sp'}, dimensions={0}, use_global_device_ids=true | all-gather | bytes 655360 | tf_op jit(solution)/shard_map/all_gather | solution.py:146
  33.0 0.6 multiply_reduce_fusion.3
  33.6 0.1 multiply_convert_fusion.3
  33.7 0.6 fusion.78
  34.4 2.5 %collective-permute-start.1 = (bf16[128,2,64]{0,2,1:T(8,128)(2,1)}, bf16[128,2,64]{0,2,1:T(8,128)(2,1)S(1)}, u32[]{:S(2)}, u32[]{:S(2)}) collective-permute-start(bf16[128,2,64]{0,2,1:T(8,128)(2,1)} %get-tuple-element.55), channel_id=1, source_target_pairs={{0,4},{4,8},{8,12},{1,5},{5,9},{9,13},{2,6},{6,10},{10,14},{3,7},{... | collective-permute-start | bytes 98312 | tf_op jit(solution)/shard_map/ppermute | solution.py:13
  36.9 18.4 %all_gather.35 = bf16[2048,128]{1,0:T(8,128)(2,1)S(1)} all-gather(bf16[512,128]{1,0:T(8,128)(2,1)S(1)} %copy-done.3), channel_id=1, replica_groups=mesh['grp'=2,'sp'=4,'tp'=4] {'sp'}, dimensions={0}, use_global_device_ids=true | all-gather | bytes 655360 | tf_op jit(solution)/shard_map/all_gather | solution.py:147
  55.3 0.6 convolution_convert_fusion.1
  55.8 0.6 fusion.77
  56.5 1.9 collective-permute-start
  58.4 0.0 all-gather.11.cloned.1.call-update
  58.4 0.0 all-gather.15.cloned.1.call-start
  58.5 0.1 reshape.180
  58.6 0.1 add_compare_fusion
  58.7 0.8 broadcast_and_fusion
  59.4 0.7 fusion.58
  60.2 1.3 slice_reduce_fusion.1
  61.5 0.1 max.16
  62.9 0.6 copy.31
  63.6 1.9 multiply_reduce_fusion.2
  65.5 13.2 %all-gather.13.cloned.1.call-done = bf16[2048,256]{1,0:T(8,128)(2,1)} async-done(((bf16[512,256]{1,0:T(8,128)(2,1)}), bf16[2048,256]{1,0:T(8,128)(2,1)}) %all-gather.13.cloned.1.call-update) | async-done | bytes 1048592 | tf_op jit(solution)/shard_map/all_gather | solution.py:145
  78.7 1.9 bitcast_reduce_fusion
  80.6 27.4 %all-gather.9.cloned.1.call-done = bf16[2048,256]{1,0:T(8,128)(2,1)} async-done(((bf16[512,256]{1,0:T(8,128)(2,1)}), bf16[2048,256]{1,0:T(8,128)(2,1)}) %all-gather.9.cloned.1.call-update) | async-done | bytes 1048592 | tf_op jit(solution)/shard_map/all_gather | solution.py:143
  108.0 1.9 multiply_reduce_fusion.1
  110.0 26.9 %all-gather.11.cloned.1.call-done = bf16[2048,256]{1,0:T(8,128)(2,1)} async-done(((bf16[512,256]{1,0:T(8,128)(2,1)}), bf16[2048,256]{1,0:T(8,128)(2,1)}) %all-gather.11.cloned.1.call-update) | async-done | bytes 1048592 | tf_op jit(solution)/shard_map/all_gather | solution.py:144
  136.8 1.9 convolution_convert_fusion
  138.7 0.1 copy.26
  138.9 15.3 %all_gather.34 = bf16[1024,2,128]{2,0,1:T(8,128)(2,1)S(1)} all-gather(bf16[256,2,128]{2,0,1:T(8,128)(2,1)S(1)} %copy.26), channel_id=1, replica_groups=mesh['grp'=2,'sp'=4,'tp'=4] {'sp'}, dimensions={0}, use_global_device_ids=true | all-gather | bytes 655360 | tf_op jit(solution)/shard_map/all_gather | solution.py:51
  154.2 0.1 multiply_convert_fusion.2
  154.3 0.1 multiply_convert_fusion.1
  154.4 15.0 %all_gather.32 = bf16[1024,2,2,64]{0,3,2,1:T(8,128)(2,1)S(1)} all-gather(bf16[256,2,2,64]{0,3,2,1:T(8,128)(2,1)S(1)} %multiply_convert_fusion.1), channel_id=1, replica_groups=mesh['grp'=2,'sp'=4,'tp'=4] {'sp'}, dimensions={0}, use_global_device_ids=true | all-gather | bytes 655360 | tf_op jit(solution)/shard_map/all_gather | solution.py:50
  169.4 0.1 reshape.181
  169.5 2.3 %conditional.2 = (f32[2,2,128]{2,1,0:T(2,128)S(1)}, f32[2,2,128,128]{2,3,0,1:T(8,128)S(1)}) conditional(s32[]{:T(128)} %convert_element_type.54, () %tuple.21, (s32[1024]{0:T(1024)S(1)}, s32[128]{0:T(128)S(1)}, bf16[256,2,2,64]{0,3,2,1:T(8,128)(2,1)S(1)}, bf16[1024,2,2,64]{0,3,2,1:T(8,128)(2,1)S(1)}, bf16[1024,2,128]{2,0,1:T(8,128)(2,1)S(1)}) %tuple.59), branch_computations={%region_4.0_spmd, %region_5.8_spmd} | conditional | flops 207224320 | bytes 8733200 | solution.py:58
  169.6 0.1 broadcast_compare_fusion
  169.7 0.6 fusion
  170.3 0.7 fusion.3
  171.1 0.6 fusion.2
  171.7 0.1 copy.43
  171.9 2.5 %conditional.3 = (f32[2,2,128]{2,1,0:T(2,128)S(1)}, f32[2,2,128,128]{2,3,0,1:T(8,128)S(1)}) conditional(s32[]{:T(128)} %convert_element_type.60, () %tuple.23, (s32[1024]{0:T(1024)S(1)}, s32[128]{0:T(128)S(1)}, bf16[256,2,2,64]{0,3,2,1:T(8,128)(2,1)S(1)}, bf16[1024,2,2,64]{0,3,2,1:T(8,128)(2,1)S(1)}, bf16[1024,2,128]{2,0,1:T(8,128)(2,1)S(1)}) %tuple.58), branch_computations={%region_9.10_spmd, %region_10.13_spmd} | conditional | flops 207224320 | bytes 8733200 | solution.py:58
  171.9 0.1 broadcast_compare_fusion.1
  172.1 0.6 fusion.14
  172.7 0.7 fusion.17
  173.4 0.6 fusion.16
  174.1 0.1 copy.45
  174.5 0.4 fusion.79
  174.9 0.1 broadcast_maximum_fusion.2
  174.9 0.2 fusion.36
  175.1 0.1 add_bitcast_fusion
  175.3 0.1 fusion.48
  175.4 0.3 fusion.35
  175.7 0.1 copy.36
  175.9 0.1 multiply_convert_fusion
  176.0 0.5 fusion.80
  176.5 0.5 copy-done.2
  177.0 1.4 fusion.28
  178.4 0.0 all-gather.15.cloned.1.call-update
  178.4 34.4 %all-gather.15.cloned.1.call-done = bf16[1024,2048]{1,0:T(8,128)(2,1)} async-done(((bf16[256,2048]{1,0:T(8,128)(2,1)}), bf16[1024,2048]{1,0:T(8,128)(2,1)}) %all-gather.15.cloned.1.call-update) | async-done | bytes 4194320 | tf_op jit(solution)/shard_map/all_gather | solution.py:178
  212.8 4.2 %reduce_sum.100 = bf16[256,2048]{1,0:T(8,128)(2,1)} reduce(bf16[4,256,2048]{2,1,0:T(8,128)(2,1)} %bitcast.107, bf16[]{:T(256)} %constant.67.clone.1), dimensions={0}, to_apply=%region_18.19 | reduce | flops 1572864 | bytes 5242882 | tf_op jit(solution)/shard_map/reduce_sum | solution.py:178
  (60 shorter events, 0.3 us)
Async XLA Ops:
  6.5 169.5 %copy-start = (bf16[256,2048]{1,0:T(8,128)(2,1)S(1)}, bf16[256,2048]{1,0:T(8,128)(2,1)}, u32[]{:S(2)}) copy-start(bf16[256,2048]{1,0:T(8,128)(2,1)} %param.36) | copy-start | bytes 3145732
  6.5 26.5 %copy-start.1 = (bf16[256,2048]{1,0:T(8,128)(2,1)S(1)}, bf16[256,2048]{1,0:T(8,128)(2,1)}, u32[]{:S(2)}) copy-start(bf16[256,2048]{1,0:T(8,128)(2,1)} %param.21) | copy-start | bytes 3145732
  6.5 26.5 %copy-start.16 = (f32[2048]{0:T(1024)S(1)}, f32[2048]{0:T(1024)}, u32[]{:S(2)}) copy-start(f32[2048]{0:T(1024)} %param.22) | copy-start | bytes 24580
  6.5 57.0 %all-gather.7.cloned.1.call-start = ((), (), s32[]{:S(2)}) async-start(), calls=%async_computation | async-start | bytes 1310720 | tf_op jit(solution)/shard_map/all_gather | solution.py:142
  7.3 71.4 %all-gather.13.cloned.1.call-start = ((), (), s32[]{:S(2)}) async-start(), calls=%async_computation.3 | async-start | bytes 1310720 | tf_op jit(solution)/shard_map/all_gather | solution.py:145
  8.0 25.6 %copy-start.9 = (f32[64]{0:T(128)S(1)}, f32[64]{0:T(128)}, u32[]{:S(2)}) copy-start(f32[64]{0:T(128)} %param.32) | copy-start | bytes 772
  8.0 100.0 %all-gather.9.cloned.1.call-start = ((), (), s32[]{:S(2)}) async-start(), calls=%async_computation.1 | async-start | bytes 1310720 | tf_op jit(solution)/shard_map/all_gather | solution.py:143
  8.8 28.1 %copy-start.3 = (bf16[512,128]{1,0:T(8,128)(2,1)S(1)}, bf16[512,128]{1,0:T(8,128)(2,1)}, u32[]{:S(2)}) copy-start(bf16[512,128]{1,0:T(8,128)(2,1)} %param.28) | copy-start | bytes 393220
  8.8 128.1 %all-gather.11.cloned.1.call-start = ((), (), s32[]{:S(2)}) async-start(), calls=%async_computation.2 | async-start | bytes 1310720 | tf_op jit(solution)/shard_map/all_gather | solution.py:144
  33.7 27.7 %copy-start.17 = (f32[4]{0:T(128)S(1)}, f32[4]{0:T(128)}, u32[]{:S(2)}) copy-start(f32[4]{0:T(128)} %param.35) | copy-start | bytes 52
  34.4 140.0 %collective-permute-start.1 = (bf16[128,2,64]{0,2,1:T(8,128)(2,1)}, bf16[128,2,64]{0,2,1:T(8,128)(2,1)S(1)}, u32[]{:S(2)}, u32[]{:S(2)}) collective-permute-start(bf16[128,2,64]{0,2,1:T(8,128)(2,1)} %get-tuple-element.55), channel_id=1, source_target_pairs={{0,4},{4,8},{8,12},{1,5},{5,9},{9,13},{2,6},{6,10},{10,14},{3,7},{... | collective-permute-start | bytes 98312 | tf_op jit(solution)/shard_map/ppermute | solution.py:13
  56.5 118.9 %collective-permute-start = (bf16[128,2,64]{0,2,1:T(8,128)(2,1)}, bf16[128,2,64]{0,2,1:T(8,128)(2,1)S(1)}, u32[]{:S(2)}, u32[]{:S(2)}) collective-permute-start(bf16[128,2,64]{0,2,1:T(8,128)(2,1)} %bitcast.13), channel_id=1, source_target_pairs={{0,4},{4,8},{8,12},{1,5},{5,9},{9,13},{2,6},{6,10},{10,14},{3,7},{... | collective-permute-start | bytes 98312 | tf_op jit(solution)/shard_map/ppermute | solution.py:13
  58.4 154.4 %all-gather.15.cloned.1.call-start = ((), (), s32[]{:S(2)}) async-start(), calls=%async_computation.4 | async-start | bytes 5242880 | tf_op jit(solution)/shard_map/all_gather | solution.py:178
  109.9 44.3 %copy-start.12 = (f32[64]{0:T(128)S(1)}, f32[64]{0:T(128)}, u32[]{:S(2)}) copy-start(f32[64]{0:T(128)} %param.29) | copy-start | bytes 772
  109.9 44.3 %copy-start.13 = (f32[64]{0:T(128)S(1)}, f32[64]{0:T(128)}, u32[]{:S(2)}) copy-start(f32[64]{0:T(128)} %param.30) | copy-start | bytes 772
  138.7 30.8 %copy-start.11 = (s32[128]{0:T(128)S(1)}, s32[128]{0:T(128)}, u32[]{:S(2)}) copy-start(s32[128]{0:T(128)} %get-tuple-element.59) | copy-start | bytes 1540
  169.5 2.3 %copy-start.10 = (s32[128]{0:T(128)S(1)}, s32[128]{0:T(128)}, u32[]{:S(2)}) copy-start(s32[128]{0:T(128)} %get-tuple-element.60) | copy-start | bytes 1540
  171.9 2.5 %copy-start.4 = (bf16[2,128,2,64]{1,3,2,0:T(8,128)(2,1)S(1)}, bf16[2,128,2,64]{1,3,2,0:T(8,128)(2,1)}, u32[]{:S(2)}) copy-start(bf16[2,128,2,64]{1,3,2,0:T(8,128)(2,1)} %fusion.58) | copy-start | bytes 196612
  171.9 2.5 %copy-start.5 = (pred[2,128,256]{1,2,0:T(8,128)(4,1)S(1)}, pred[2,128,256]{1,2,0:T(8,128)(4,1)}, u32[]{:S(2)}) copy-start(pred[2,128,256]{1,2,0:T(8,128)(4,1)} %broadcast_and_fusion) | copy-start | bytes 196612
  171.9 2.5 %copy-start.8 = (bf16[1,128,2,64]{1,3,2,0:T(8,128)(2,1)S(1)}, bf16[1,128,2,64]{1,3,2,0:T(8,128)(2,1)}, u32[]{:S(2)}) copy-start(bf16[1,128,2,64]{1,3,2,0:T(8,128)(2,1)} %get-tuple-element.56) | copy-start | bytes 98308
  171.9 2.5 %copy-start.18 = (f32[64]{0:T(128)S(1)}, f32[64]{0:T(128)}, u32[]{:S(2)}) copy-start(f32[64]{0:T(128)} %param.31) | copy-start | bytes 772
  174.4 0.9 copy-start.15
  174.4 1.0 copy-start.6
  174.5 1.0 copy-start.7
  175.2 0.7 copy-start.14
  175.7 1.2 copy-start.2
Sparse Core Ops, SparseCore 0:
  8.9 39.4 all-gather.6
  50.0 28.6 all-gather.12
  80.3 27.6 all-gather.8
  109.4 27.3 all-gather.10
  178.5 34.2 all-gather.14
